TPU v7x, 32 devices: a whole 2x2x4 slice. The times are simulated.
32 devices in a mesh: sp: 8 (over z, x), dp: 4 (over y, core).
Axes of the slice: x: 2, y: 2, z: 4, core: 2. Of those that a mesh axis runs over, the one named last changes fastest.
Arguments:
- tokens: bfloat16 [4, 4096, 2048], P('dp', 'sp'), may hold values from -6 to 6
- segments: int32 [4, 4096], P('dp', 'sp'), may hold values from 0 to 3, never falling along the last dimension, each value on 1 to 2048 neighbouring positions
- w_lin: bfloat16 [2048, 1024], P('dp'), may hold values from -0.125 to 0.125
- w_gate: bfloat16 [2048, 1024], P('dp'), may hold values from -0.125 to 0.125
- w_out: bfloat16 [1024, 2048], P(None, 'dp'), may hold values from -0.1875 to 0.1875
- conv_kernel: float32 [31, 1024], replicated, may hold values from -1 to 1
- conv_bias: float32 [1024], replicated, may hold values from -3 to 3
- norm_gain: float32 [1024], replicated, may hold values from 0.1 to 1.9
- norm_bias: float32 [1024], replicated, may hold values from -3 to 3
Outputs:
- mixed_out: bfloat16 [4, 4096, 2048], P('dp', 'sp')
Inputs may be any that keep to these rules, and one draw needn't show every extreme that they name: `segments`: within each sequence document numbers never fall; a document is a run of equal numbers of at most four times 512 positions.
All inputs are finite; a program needn't handle non-finite values.
Results may differ from a plain program's by a relative error of at most 0.0062.
Values may be sent and summed in bfloat16 or wider, within the bound.
No kernel may reach another device: no remote copies, remote signals or barrier semaphores. Data moves between devices by JAX's collectives and lax.ppermute only.
A program may use at most 64 MiB of HBM per device.

v0:
```python
import jax
import jax.numpy as jnp
from jax import lax
from jax.sharding import PartitionSpec as P

K = 31


def from_behind(value, axis, by):
    devices = lax.axis_size(axis)
    pairs = [(i, i + by) for i in range(devices) if 0 <= i + by < devices]
    return lax.ppermute(value, axis, pairs)


def conv_doc(values, doc_ids, kernel, bias):
    taps = kernel.shape[0]
    reach = taps - 1
    length = values.shape[1]
    place = lax.iota(jnp.int32, length)
    change = jnp.concatenate([jnp.ones((1,), jnp.bool_), doc_ids[1:] != doc_ids[:-1]])
    begins = lax.cummax(jnp.where(change, place, 0), axis=0)[reach:]
    here = place[reach:]
    total = bias[:, None] + kernel[reach][:, None] * values[:, reach:].astype(jnp.float32)
    for back in range(1, taps):
        piece = values[:, reach - back : length - back].astype(jnp.float32)
        keep = here - back >= begins
        total = total + kernel[reach - back][:, None] * jnp.where(keep[None, :], piece, 0.0)
    return total


def body(tokens, segments, w_lin, w_gate, w_out, conv_kernel, conv_bias, norm_gain, norm_bias):
    rows = tokens[0]
    doc_ids = segments[0]
    count = rows.shape[0]
    reach = K - 1
    first = jnp.einsum(
        "rc,tr->ct",
        lax.all_gather(w_lin, "dp", axis=0, tiled=True),
        rows,
        preferred_element_type=jnp.float32,
    )
    second = jnp.einsum(
        "rc,tr->ct",
        lax.all_gather(w_gate, "dp", axis=0, tiled=True),
        rows,
        preferred_element_type=jnp.float32,
    )
    glu = (first * jax.nn.sigmoid(second)).astype(jnp.bfloat16)
    tail, tail_ids = from_behind((glu[:, count - reach :], doc_ids[count - reach :]), "sp", 1)
    extended = jnp.concatenate([tail, glu], axis=1)
    ext_ids = jnp.concatenate([tail_ids, doc_ids], axis=0)
    conv = conv_doc(extended, ext_ids, conv_kernel, conv_bias)
    conved = lax.optimization_barrier(conv.astype(jnp.bfloat16))
    values = conved.astype(jnp.float32)
    mean = jnp.mean(values, axis=0, keepdims=True)
    var = jnp.mean(jnp.square(values - mean), axis=0, keepdims=True)
    normed = (values - mean) * lax.rsqrt(var + 1e-05) * norm_gain[:, None] + norm_bias[:, None]
    act = jax.nn.silu(normed).astype(jnp.bfloat16)
    mixed_out = jnp.einsum(
        "ct,cr->tr",
        act,
        lax.all_gather(w_out, "dp", axis=1, tiled=True),
        preferred_element_type=jnp.float32,
    ).astype(jnp.bfloat16)
    return mixed_out[None]


def solution(mesh):
    placed = (
        P("dp", "sp", None),
        P("dp", "sp"),
        P("dp", None),
        P("dp", None),
        P(None, "dp"),
        P(),
        P(),
        P(),
        P(),
    )
    return jax.shard_map(
        body, mesh=mesh, in_specs=placed, out_specs=P("dp", "sp", None), check_vma=False
    )
```

profile of v0, /device:TPU:0, one launch (start us, length us, event | category | flops | bytes accessed | tf_op | source)
XLA Modules:
  0.0 131.1 jit_solution(17335974425128062268)
XLA Ops:
  6.5 0.7 all-gather.4.cloned.1.call-update
  7.3 0.0 all-gather.6.cloned.1.call-start
  7.3 0.7 all-gather.6.cloned.1.call-update
  8.0 0.0 all-gather.8.cloned.1.call-start
  8.1 0.1 slice_bitcast_fusion
  8.1 4.9 %collective-permute-start = (s32[30]{0:T(128)S(1)}, s32[30]{0:T(128)S(1)}, u32[]{:S(2)}, u32[]{:S(2)}) collective-permute-start(s32[30]{0:T(128)S(1)} %slice_bitcast_fusion), channel_id=1, source_target_pairs={{0,4},{4,8},{8,12},{12,16},{16,20},{20,24},{24,28},{1,5},{5,9},{9,... | collective-permute-start | bytes 368 | tf_op jit(solution)/shard_map/ppermute | solution.py:12
  13.0 0.0 all-gather.8.cloned.1.call-update
  13.0 0.1 fusion.54
  13.2 1.1 collective-permute-done
  14.3 0.1 pad_add_fusion
  14.4 0.1 slice_compare_fusion
  14.4 0.1 iota_select_fusion
  14.5 0.3 reduce-window.9
  14.8 0.1 slice.278
  14.9 0.1 slice_reduce_fusion
  15.0 0.1 maximum_bitcast_fusion
  15.1 0.1 add_compare_fusion.20
  15.2 0.1 add_compare_fusion.11
  15.3 0.1 add_compare_fusion.29
  15.3 30.8 %all-gather.4.cloned.1.call-done = bf16[2048,1024]{1,0:T(8,128)(2,1)} async-done(((bf16[512,1024]{1,0:T(8,128)(2,1)}), bf16[2048,1024]{1,0:T(8,128)(2,1)}) %all-gather.4.cloned.1.call-update) | async-done | bytes 4194320 | tf_op jit(solution)/shard_map/all_gather | solution.py:38
  46.1 0.0 copy-done
  46.1 5.8 %fusion.12 = f32[1024,512]{0,1:T(8,128)} fusion(bf16[2048,1024]{1,0:T(8,128)(2,1)} %all-gather.4.cloned.1.call-done, bf16[1,512,2048]{2,1,0:T(8,128)(2,1)S(1)} %copy-done), kind=kOutput, calls=%fused_computation.44 | convolution fusion | flops 2147483648 | bytes 8388608 | tf_op jit(solution)/shard_map/rc,tr->ct/dot_general | solution.py:36
  52.0 30.2 %all-gather.6.cloned.1.call-done = bf16[2048,1024]{1,0:T(8,128)(2,1)} async-done(((bf16[512,1024]{1,0:T(8,128)(2,1)}), bf16[2048,1024]{1,0:T(8,128)(2,1)}) %all-gather.6.cloned.1.call-update) | async-done | bytes 4194320 | tf_op jit(solution)/shard_map/all_gather | solution.py:44
  82.2 5.4 %multiply_convert_fusion = bf16[1024,512]{0,1:T(8,128)(2,1)S(1)} fusion(f32[1024,512]{0,1:T(8,128)} %fusion.12, bf16[2048,1024]{1,0:T(8,128)(2,1)} %all-gather.6.cloned.1.call-done, bf16[1,512,2048]{2,1,0:T(8,128)(2,1)S(1)} %copy-done), kind=kOutput, calls=%fused_computation.49 | convolution fusion | flops 2150105088 | bytes 9437184 | tf_op jit(solution)/shard_map/rc,tr->ct/dot_general | solution.py:42
  87.6 3.4 %collective-permute-start.1 = (bf16[1024,30]{0,1:T(8,128)(2,1)S(1)}, bf16[1024,30]{0,1:T(8,128)(2,1)S(1)}, u32[]{:S(2)}, u32[]{:S(2)}) collective-permute-start(bf16[1024,30]{0,1:T(8,128)(2,1)S(1)} %slice.341), channel_id=1, source_target_pairs={{0,4},{4,8},{8,12},{12,16},{16,20},{20,24},{24,28},{1,5},{5,9},{9,... | collective-permute-start | bytes 184328 | tf_op jit(solution)/shard_map/ppermute | solution.py:12
  91.0 0.1 add_compare_fusion.2
  91.1 1.8 %collective-permute-done.1 = bf16[1024,30]{0,1:T(8,128)(2,1)S(1)} collective-permute-done((bf16[1024,30]{0,1:T(8,128)(2,1)S(1)}, bf16[1024,30]{0,1:T(8,128)(2,1)S(1)}, u32[]{:S(2)}, u32[]{:S(2)}) %collective-permute-start.1) | collective-permute-done | bytes 61472 | tf_op jit(solution)/shard_map/ppermute | solution.py:12
  92.9 15.9 %add_convert_fusion = bf16[1024,512]{0,1:T(8,128)(2,1)S(1)} fusion(bf16[1024,512]{0,1:T(8,128)(2,1)S(1)} %multiply_convert_fusion, bf16[1024,30]{0,1:T(8,128)(2,1)S(1)} %collective-permute-done.1, f32[1024]{0:T(1024)S(1)} %bitcast.79, f32[1024]{0:T(1024)S(1)} %bitcast.80, f32[1024]{0:T(1024)S(1)} %bitcast.51, f32[1024]{0:T(1024)S(1)} %bitcast.52, ...), kind=kLoop, calls=%fused_computation.48 | loop fusion | flops 112197632 | bytes 2305024 | tf_op jit(solution)/shard_map/convert_element_type | solution.py:53
  108.8 0.2 convert_reduce_fusion
  109.0 0.4 fusion.3
  109.5 8.8 %all-gather.8.cloned.1.call-done = bf16[1024,2048]{1,0:T(8,128)(2,1)} async-done(((bf16[1024,512]{1,0:T(8,128)(2,1)}), bf16[1024,2048]{1,0:T(8,128)(2,1)}) %all-gather.8.cloned.1.call-update) | async-done | bytes 4194320 | tf_op jit(solution)/shard_map/all_gather | solution.py:62
  118.2 6.3 %fusion = bf16[1,512,2048]{2,1,0:T(8,128)(2,1)} fusion(bf16[1024,2048]{1,0:T(8,128)(2,1)} %all-gather.8.cloned.1.call-done, bf16[1024,512]{0,1:T(8,128)(2,1)S(1)} %add_convert_fusion, f32[1024]{0:T(1024)S(1)} %copy-done.4, f32[1024]{0:T(1024)S(1)} %copy-done.5, f32[512]{0:T(512)S(1)} %add_rsqrt_fusion, f32[512]{0:T(512)S(1)} %broadcast_multiply_fusion), kind=kOutput, calls=%fused_computation.30 | convolution fusion | flops 2153775104 | bytes 7352320 | tf_op jit(solution)/shard_map/ct,cr->tr/dot_general | solution.py:59
  (19 shorter events, 0.1 us)
Async XLA Ops:
  6.5 39.6 %copy-start = (bf16[1,512,2048]{2,1,0:T(8,128)(2,1)S(1)}, bf16[1,512,2048]{2,1,0:T(8,128)(2,1)}, u32[]{:S(2)}) copy-start(bf16[1,512,2048]{2,1,0:T(8,128)(2,1)} %param.9) | copy-start | bytes 6291460
  6.5 1.5 %copy-start.3 = (s32[1,512]{1,0:T(1,128)S(1)}, s32[1,512]{1,0:T(1,128)}, u32[]{:S(2)}) copy-start(s32[1,512]{1,0:T(1,128)} %param.10) | copy-start | bytes 6148
  6.5 6.5 %copy-start.1 = (f32[31,1024]{1,0:T(8,128)S(1)}, f32[31,1024]{1,0:T(8,128)}, u32[]{:S(2)}) copy-start(f32[31,1024]{1,0:T(8,128)} %param.14) | copy-start | bytes 380932
  6.5 39.6 %all-gather.4.cloned.1.call-start = ((), (), s32[]{:S(2)}) async-start(), calls=%async_computation | async-start | bytes 5242880 | tf_op jit(solution)/shard_map/all_gather | solution.py:38
  7.3 74.9 %all-gather.6.cloned.1.call-start = ((), (), s32[]{:S(2)}) async-start(), calls=%async_computation.1 | async-start | bytes 5242880 | tf_op jit(solution)/shard_map/all_gather | solution.py:44
  8.0 110.2 %all-gather.8.cloned.1.call-start = ((), (), s32[]{:S(2)}) async-start(), calls=%async_computation.2 | async-start | bytes 5242880 | tf_op jit(solution)/shard_map/all_gather | solution.py:62
  8.1 6.1 %collective-permute-start = (s32[30]{0:T(128)S(1)}, s32[30]{0:T(128)S(1)}, u32[]{:S(2)}, u32[]{:S(2)}) collective-permute-start(s32[30]{0:T(128)S(1)} %slice_bitcast_fusion), channel_id=1, source_target_pairs={{0,4},{4,8},{8,12},{12,16},{16,20},{20,24},{24,28},{1,5},{5,9},{9,... | collective-permute-start | bytes 368 | tf_op jit(solution)/shard_map/ppermute | solution.py:12
  52.0 40.9 %copy-start.2 = (f32[1024]{0:T(1024)S(1)}, f32[1024]{0:T(1024)}, u32[]{:S(2)}) copy-start(f32[1024]{0:T(1024)} %param.15) | copy-start | bytes 12292
  87.6 5.3 %collective-permute-start.1 = (bf16[1024,30]{0,1:T(8,128)(2,1)S(1)}, bf16[1024,30]{0,1:T(8,128)(2,1)S(1)}, u32[]{:S(2)}, u32[]{:S(2)}) collective-permute-start(bf16[1024,30]{0,1:T(8,128)(2,1)S(1)} %slice.341), channel_id=1, source_target_pairs={{0,4},{4,8},{8,12},{12,16},{16,20},{20,24},{24,28},{1,5},{5,9},{9,... | collective-permute-start | bytes 184328 | tf_op jit(solution)/shard_map/ppermute | solution.py:12
  92.9 25.3 %copy-start.4 = (f32[1024]{0:T(1024)S(1)}, f32[1024]{0:T(1024)}, u32[]{:S(2)}) copy-start(f32[1024]{0:T(1024)} %param.17) | copy-start | bytes 12292
  92.9 25.3 %copy-start.5 = (f32[1024]{0:T(1024)S(1)}, f32[1024]{0:T(1024)}, u32[]{:S(2)}) copy-start(f32[1024]{0:T(1024)} %param.16) | copy-start | bytes 12292
Sparse Core Ops, SparseCore 0:
  8.9 37.1 all-gather.3
  47.7 34.4 all-gather.5
  83.7 34.4 all-gather.7
where the time goes:
time: 131 us
  waiting for transfers between devices  74.1 us (57%)
  matrix products  17.6 us (13%)
  other arithmetic  17.5 us (13%)
  between operations  13.2 us (10%)
  starting transfers between devices  8.31 us (6%)
    all_gather x1, waiting for transfers between devices, body(): lax.all_gather(w_lin, 'dp', axis=0, tiled=True)  30.8 us
    all_gather x1, waiting for transfers between devices, body(): lax.all_gather(w_gate, 'dp', axis=0, tiled=True)  30.2 us
    convert_element_type x1, other arithmetic, body(): conved = lax.optimization_barrier(conv.astype(jnp.bfloat16))  15.9 us
    all_gather x1, waiting for transfers between devices, body(): lax.all_gather(w_out, 'dp', axis=1, tiled=True)  8.75 us
    ppermute x2, starting transfers between devices, from_behind(): return lax.ppermute(value, axis, pairs)  8.23 us
    dot_general x1, matrix products, body(): jnp.einsum('ct,cr->tr', act, lax.all_gather(w_out, 'dp', axis=1, tiled=Tr...  6.35 us
    dot_general x1, matrix products, body(): jnp.einsum('rc,tr->ct', lax.all_gather(w_lin, 'dp', axis=0, tiled=True),...  5.84 us
    dot_general x1, matrix products, body(): jnp.einsum('rc,tr->ct', lax.all_gather(w_gate, 'dp', axis=0, tiled=True),...  5.44 us
  transfers between devices with their start and end apart: 5, of which 5 were waited for; matrix products, arithmetic and copies ran while one was open for 22% of the time, Pallas kernels for 0%

commit v1 on v0

--- a/solution.py
+++ b/solution.py
@@ -2,6 +2,7 @@
 import jax.numpy as jnp
 from jax import lax
 from jax.sharding import PartitionSpec as P
+from jax.lax import axis_index, axis_size, ppermute
 
 K = 31
 
@@ -29,15 +30,35 @@
 
 
 def body(tokens, segments, w_lin, w_gate, w_out, conv_kernel, conv_bias, norm_gain, norm_bias):
+
+    def squares_remake(own_rows, x_in):
+        raw_out = axis_size("dp")
+        arr_next = axis_index("dp")
+        extra, small = (raw_out, arr_next)
+        seen = tuple(((ii, (ii - 1) % extra) for ii in range(extra)))
+        h_now = own_rows.shape[0]
+        e_next = own_rows
+        finding = x_in(e_next, small * h_now)
+        i0 = 1
+        while i0 < extra:
+            e_next = ppermute(e_next, "dp", perm=seen)
+            earlier = x_in(e_next, (small + i0) % extra * h_now)
+            finding = finding + earlier
+            i0 += 1
+        return finding
+
     rows = tokens[0]
     doc_ids = segments[0]
     count = rows.shape[0]
     reach = K - 1
-    first = jnp.einsum(
-        "rc,tr->ct",
-        lax.all_gather(w_lin, "dp", axis=0, tiled=True),
-        rows,
-        preferred_element_type=jnp.float32,
+    first = squares_remake(
+        w_lin,
+        lambda shard, at: jnp.einsum(
+            "rc,tr->ct",
+            shard,
+            lax.dynamic_slice_in_dim(rows, at, shard.shape[0], axis=1),
+            preferred_element_type=jnp.float32,
+        ),
     )
     second = jnp.einsum(
         "rc,tr->ct",

time: 131 us -> 118 us (0.901); the launches traced: 131 us -> 117 us
  waiting for transfers between devices: 74.1 us -> 50.5 us
  starting transfers between devices: 8.31 us -> 12.8 us
  matrix products: 17.6 us -> 21.2 us
    ppermute x0 -> x3, waiting for transfers between devices: none -> 48 us  [squares_remake(): e_next = ppermute(e_next, 'dp', perm=seen)]
    all_gather x1 -> x0, waiting for transfers between devices: 30.8 us -> none  [body(): lax.all_gather(w_lin, 'dp', axis=0, tiled=True)]
    all_gather x1, waiting for transfers between devices: 30.2 us -> 0.01 us  [body(): lax.all_gather(w_gate, 'dp', axis=0, tiled=True)]
    all_gather x1, waiting for transfers between devices: 8.75 us -> 0.02 us  [body(): lax.all_gather(w_out, 'dp', axis=1, tiled=True)]
    ppermute x0 -> x3, starting transfers between devices: none -> 6.49 us  [squares_remake(): e_next = ppermute(e_next, 'dp', perm=seen)]
    dot_general x1 -> x4, matrix products: 5.84 us -> 9.69 us  [body(): jnp.einsum('rc,tr->ct', shard, lax.dynamic_slice_in_dim(rows, at, shard.s...]
    ppermute x2, starting transfers between devices: 8.23 us -> 6.32 us  [from_behind(): return lax.ppermute(value, axis, pairs)]
  transfers between devices with their start and end apart: 5 -> 7, of which waited for: 5 -> 4; matrix products, arithmetic and copies ran while one was open for 22% -> 29% of each run, Pallas kernels for 0% -> 0%
where the time goes in v1:
time: 118 us; the launch traced here: 117 us
  waiting for transfers between devices  50.5 us (43%)
  matrix products  21.2 us (18%)
  other arithmetic  17.5 us (15%)
  between operations  13.6 us (12%)
  starting transfers between devices  12.8 us (11%)
    ppermute x3, waiting for transfers between devices, squares_remake(): e_next = ppermute(e_next, 'dp', perm=seen)  48 us
    convert_element_type x1, other arithmetic, body(): conved = lax.optimization_barrier(conv.astype(jnp.bfloat16))  15.9 us
    dot_general x4, matrix products, body(): jnp.einsum('rc,tr->ct', shard, lax.dynamic_slice_in_dim(rows, at, shard.s...  9.69 us
    ppermute x3, starting transfers between devices, squares_remake(): e_next = ppermute(e_next, 'dp', perm=seen)  6.49 us
    dot_general x1, matrix products, body(): jnp.einsum('ct,cr->tr', act, lax.all_gather(w_out, 'dp', axis=1, tiled=Tr...  6.34 us
    ppermute x2, starting transfers between devices, from_behind(): return lax.ppermute(value, axis, pairs)  6.32 us
    dot_general x1, matrix products, body(): jnp.einsum('rc,tr->ct', lax.all_gather(w_gate, 'dp', axis=0, tiled=True),...  5.13 us
  transfers between devices with their start and end apart: 7, of which 4 were waited for; matrix products, arithmetic and copies ran while one was open for 29% of the time, Pallas kernels for 0%

profile of v1, /device:TPU:0, one launch (start us, length us, event | category | flops | bytes accessed | tf_op | source)
XLA Modules:
  0.0 116.7 jit_solution(3166367386002997402)
XLA Ops:
  6.5 0.7 all-gather.3.cloned.1.call-update
  7.3 2.5 %collective-permute-start = (bf16[512,1024]{1,0:T(8,128)(2,1)}, bf16[512,1024]{1,0:T(8,128)(2,1)}, u32[]{:S(2)}, u32[]{:S(2)}) collective-permute-start(bf16[512,1024]{1,0:T(8,128)(2,1)} %param.11), channel_id=1, source_target_pairs={{0,3},{1,0},{2,1},{3,2},{4,7},{5,4},{6,5},{7,6},{8,11},{9,8},{10,9... | collective-permute-start | bytes 3145736 | tf_op jit(solution)/shard_map/ppermute | solution.py:44
  9.8 0.7 slice_bitcast_fusion
  10.5 3.4 %collective-permute-start.3 = (s32[30]{0:T(128)S(1)}, s32[30]{0:T(128)S(1)}, u32[]{:S(2)}, u32[]{:S(2)}) collective-permute-start(s32[30]{0:T(128)S(1)} %slice_bitcast_fusion), channel_id=1, source_target_pairs={{0,4},{4,8},{8,12},{12,16},{16,20},{20,24},{24,28},{1,5},{5,9},{9,... | collective-permute-start | bytes 368 | tf_op jit(solution)/shard_map/ppermute | solution.py:13
  14.1 0.1 fusion.66
  14.1 2.1 %fusion.55 = f32[512,1024]{1,0:T(8,128)} fusion(bf16[512,1024]{1,0:T(8,128)(2,1)S(1)} %copy-done.4, bf16[1,512,2048]{2,1,0:T(8,128)(2,1)S(1)} %copy-done, s32[]{:T(128)S(6)} %select_n.122), kind=kOutput, calls=%fused_computation.94 | convolution fusion | flops 536870912 | bytes 3670020 | tf_op jit(solution)/shard_map/rc,tr->ct/dot_general | solution.py:56
  16.3 0.1 pad_add_fusion
  16.3 0.1 slice_compare_fusion
  16.4 0.1 iota_select_fusion
  16.5 10.7 %collective-permute-done = bf16[512,1024]{1,0:T(8,128)(2,1)} collective-permute-done((bf16[512,1024]{1,0:T(8,128)(2,1)}, bf16[512,1024]{1,0:T(8,128)(2,1)}, u32[]{:S(2)}, u32[]{:S(2)}) %collective-permute-start) | collective-permute-done | bytes 1048608 | tf_op jit(solution)/shard_map/ppermute | solution.py:44
  27.1 2.2 %collective-permute-start.1 = (bf16[512,1024]{1,0:T(8,128)(2,1)}, bf16[512,1024]{1,0:T(8,128)(2,1)S(1)}, u32[]{:S(2)}, u32[]{:S(2)}) collective-permute-start(bf16[512,1024]{1,0:T(8,128)(2,1)} %collective-permute-done), channel_id=1, source_target_pairs={{0,3},{1,0},{2,1},{3,2},{4,7},{5,4},{6,5},{7,6},{8,11},{9,8},{10,9... | collective-permute-start | bytes 3145736 | tf_op jit(solution)/shard_map/ppermute | solution.py:44
  29.3 0.3 reduce-window.9
  29.6 0.1 slice.278
  29.7 0.1 slice_reduce_fusion
  29.8 0.1 maximum_bitcast_fusion
  29.9 0.1 add_compare_fusion.29
  30.0 0.1 add_compare_fusion.20
  30.1 0.1 add_compare_fusion.11
  30.2 26.0 %collective-permute-done.1 = bf16[512,1024]{1,0:T(8,128)(2,1)S(1)} collective-permute-done((bf16[512,1024]{1,0:T(8,128)(2,1)}, bf16[512,1024]{1,0:T(8,128)(2,1)S(1)}, u32[]{:S(2)}, u32[]{:S(2)}) %collective-permute-start.1) | collective-permute-done | bytes 1048608 | tf_op jit(solution)/shard_map/ppermute | solution.py:44
  56.1 1.8 %collective-permute-start.2 = (bf16[512,1024]{1,0:T(8,128)(2,1)S(1)}, bf16[512,1024]{1,0:T(8,128)(2,1)}, u32[]{:S(2)}, u32[]{:S(2)}) collective-permute-start(bf16[512,1024]{1,0:T(8,128)(2,1)S(1)} %collective-permute-done.1), channel_id=1, source_target_pairs={{0,3},{1,0},{2,1},{3,2},{4,7},{5,4},{6,5},{7,6},{8,11},{9,8},{10,9... | collective-permute-start | bytes 3145736 | tf_op jit(solution)/shard_map/ppermute | solution.py:44
  57.9 3.3 %fusion.53 = f32[512,1024]{1,0:T(8,128)} fusion(bf16[512,1024]{1,0:T(8,128)(2,1)} %collective-permute-done, bf16[1,512,2048]{2,1,0:T(8,128)(2,1)S(1)} %copy-done, s32[]{:T(128)S(6)} %select_n.124), kind=kOutput, calls=%fused_computation.92 | convolution fusion | flops 536870912 | bytes 3670020 | tf_op jit(solution)/shard_map/rc,tr->ct/dot_general | solution.py:56
  61.2 2.0 %fusion.51 = f32[512,1024]{1,0:T(8,128)} fusion(bf16[512,1024]{1,0:T(8,128)(2,1)S(1)} %collective-permute-done.1, bf16[1,512,2048]{2,1,0:T(8,128)(2,1)S(1)} %copy-done, s32[]{:T(128)S(6)} %select_n.126), kind=kOutput, calls=%fused_computation.90 | convolution fusion | flops 536870912 | bytes 3670020 | tf_op jit(solution)/shard_map/rc,tr->ct/dot_general | solution.py:56
  63.3 5.1 %fusion.12 = f32[1024,512]{0,1:T(8,128)S(1)} fusion(bf16[2048,1024]{1,0:T(8,128)(2,1)} %all-gather.3.cloned.1.call-done, bf16[1,512,2048]{2,1,0:T(8,128)(2,1)S(1)} %copy-done), kind=kOutput, calls=%fused_computation.44 | convolution fusion | flops 2147483648 | bytes 8388608 | tf_op jit(solution)/shard_map/rc,tr->ct/dot_general | solution.py:63
  68.4 11.3 %collective-permute-done.2 = bf16[512,1024]{1,0:T(8,128)(2,1)} collective-permute-done((bf16[512,1024]{1,0:T(8,128)(2,1)S(1)}, bf16[512,1024]{1,0:T(8,128)(2,1)}, u32[]{:S(2)}, u32[]{:S(2)}) %collective-permute-start.2) | collective-permute-done | bytes 1048608 | tf_op jit(solution)/shard_map/ppermute | solution.py:44
  79.7 2.3 %fusion.14 = bf16[1024,512]{0,1:T(8,128)(2,1)S(1)} fusion(f32[1024,512]{0,1:T(8,128)S(1)} %fusion.12, f32[512,1024]{1,0:T(8,128)S(1)} %copy-done.3, f32[512,1024]{1,0:T(8,128)S(1)} %copy-done.1, f32[512,1024]{1,0:T(8,128)S(1)} %copy-done.2, bf16[512,1024]{1,0:T(8,128)(2,1)} %collective-permute-done.2, bf16[1,512,2048]{2,1,0:T(8,128)(2,1)S(1)} %copy-done, ...), kind=kOutput, calls=%fused_computation.47 | convolution fusion | flops 541065216 | bytes 11010052 | tf_op jit(solution)/shard_map/rc,tr->ct/dot_general | solution.py:56
  82.1 2.9 %collective-permute-start.4 = (bf16[1024,30]{0,1:T(8,128)(2,1)S(1)}, bf16[1024,30]{0,1:T(8,128)(2,1)S(1)}, u32[]{:S(2)}, u32[]{:S(2)}) collective-permute-start(bf16[1024,30]{0,1:T(8,128)(2,1)S(1)} %slice.341), channel_id=1, source_target_pairs={{0,4},{4,8},{8,12},{12,16},{16,20},{20,24},{24,28},{1,5},{5,9},{9,... | collective-permute-start | bytes 184328 | tf_op jit(solution)/shard_map/ppermute | solution.py:13
  85.0 0.1 add_compare_fusion.2
  85.1 1.8 %collective-permute-done.4 = bf16[1024,30]{0,1:T(8,128)(2,1)S(1)} collective-permute-done((bf16[1024,30]{0,1:T(8,128)(2,1)S(1)}, bf16[1024,30]{0,1:T(8,128)(2,1)S(1)}, u32[]{:S(2)}, u32[]{:S(2)}) %collective-permute-start.4) | collective-permute-done | bytes 61472 | tf_op jit(solution)/shard_map/ppermute | solution.py:13
  86.9 15.9 %add_convert_fusion = bf16[1024,512]{0,1:T(8,128)(2,1)S(1)} fusion(bf16[1024,512]{0,1:T(8,128)(2,1)S(1)} %fusion.14, bf16[1024,30]{0,1:T(8,128)(2,1)S(1)} %collective-permute-done.4, f32[1024]{0:T(1024)S(1)} %bitcast.75, f32[1024]{0:T(1024)S(1)} %bitcast.76, f32[1024]{0:T(1024)S(1)} %bitcast.78, f32[1024]{0:T(1024)S(1)} %bitcast.79, f32[1024]{0:T(1024)S(1)} %bitcast.80, ...), kind=kLoop, calls=%fused_computation.48 | loop fusion | flops 112197632 | bytes 2305024 | tf_op jit(solution)/shard_map/convert_element_type | solution.py:74
  102.8 0.2 convert_reduce_fusion
  103.1 0.4 fusion.3
  103.5 6.3 %fusion = bf16[1,512,2048]{2,1,0:T(8,128)(2,1)} fusion(bf16[1024,2048]{1,0:T(8,128)(2,1)} %all-gather.5.cloned.1.call-done, bf16[1024,512]{0,1:T(8,128)(2,1)S(1)} %add_convert_fusion, f32[1024]{0:T(1024)S(1)} %copy-done.8, f32[1024]{0:T(1024)S(1)} %copy-done.9, f32[512]{0:T(512)S(1)} %add_rsqrt_fusion, f32[512]{0:T(512)S(1)} %broadcast_multiply_fusion), kind=kOutput, calls=%fused_computation.30 | convolution fusion | flops 2153775104 | bytes 7352320 | tf_op jit(solution)/shard_map/ct,cr->tr/dot_general | solution.py:80
  (33 shorter events, 0.2 us)
Async XLA Ops:
  6.5 7.6 %copy-start = (bf16[1,512,2048]{2,1,0:T(8,128)(2,1)S(1)}, bf16[1,512,2048]{2,1,0:T(8,128)(2,1)}, u32[]{:S(2)}) copy-start(bf16[1,512,2048]{2,1,0:T(8,128)(2,1)} %param.9) | copy-start | bytes 6291460
  6.5 7.6 %copy-start.4 = (bf16[512,1024]{1,0:T(8,128)(2,1)S(1)}, bf16[512,1024]{1,0:T(8,128)(2,1)}, u32[]{:S(2)}) copy-start(bf16[512,1024]{1,0:T(8,128)(2,1)} %param.11) | copy-start | bytes 3145732
  6.5 7.4 %copy-start.5 = (f32[31,1024]{1,0:T(8,128)S(1)}, f32[31,1024]{1,0:T(8,128)}, u32[]{:S(2)}) copy-start(f32[31,1024]{1,0:T(8,128)} %param.14) | copy-start | bytes 380932
  6.5 56.7 %all-gather.3.cloned.1.call-start = ((), (), s32[]{:S(2)}) async-start(), calls=%async_computation | async-start | bytes 5242880 | tf_op jit(solution)/shard_map/all_gather | solution.py:65
  7.3 96.2 %all-gather.5.cloned.1.call-start = ((), (), s32[]{:S(2)}) async-start(), calls=%async_computation.1 | async-start | bytes 5242880 | tf_op jit(solution)/shard_map/all_gather | solution.py:83
  7.3 19.8 %collective-permute-start = (bf16[512,1024]{1,0:T(8,128)(2,1)}, bf16[512,1024]{1,0:T(8,128)(2,1)}, u32[]{:S(2)}, u32[]{:S(2)}) collective-permute-start(bf16[512,1024]{1,0:T(8,128)(2,1)} %param.11), channel_id=1, source_target_pairs={{0,3},{1,0},{2,1},{3,2},{4,7},{5,4},{6,5},{7,6},{8,11},{9,8},{10,9... | collective-permute-start | bytes 3145736 | tf_op jit(solution)/shard_map/ppermute | solution.py:44
  10.5 5.7 %collective-permute-start.3 = (s32[30]{0:T(128)S(1)}, s32[30]{0:T(128)S(1)}, u32[]{:S(2)}, u32[]{:S(2)}) collective-permute-start(s32[30]{0:T(128)S(1)} %slice_bitcast_fusion), channel_id=1, source_target_pairs={{0,4},{4,8},{8,12},{12,16},{16,20},{20,24},{24,28},{1,5},{5,9},{9,... | collective-permute-start | bytes 368 | tf_op jit(solution)/shard_map/ppermute | solution.py:13
  13.9 2.3 %copy-start.7 = (s32[1,512]{1,0:T(1,128)S(1)}, s32[1,512]{1,0:T(1,128)}, u32[]{:S(2)}) copy-start(s32[1,512]{1,0:T(1,128)} %param.10) | copy-start | bytes 6148
  27.1 29.0 %collective-permute-start.1 = (bf16[512,1024]{1,0:T(8,128)(2,1)}, bf16[512,1024]{1,0:T(8,128)(2,1)S(1)}, u32[]{:S(2)}, u32[]{:S(2)}) collective-permute-start(bf16[512,1024]{1,0:T(8,128)(2,1)} %collective-permute-done), channel_id=1, source_target_pairs={{0,3},{1,0},{2,1},{3,2},{4,7},{5,4},{6,5},{7,6},{8,11},{9,8},{10,9... | collective-permute-start | bytes 3145736 | tf_op jit(solution)/shard_map/ppermute | solution.py:44
  56.1 23.6 %collective-permute-start.2 = (bf16[512,1024]{1,0:T(8,128)(2,1)S(1)}, bf16[512,1024]{1,0:T(8,128)(2,1)}, u32[]{:S(2)}, u32[]{:S(2)}) collective-permute-start(bf16[512,1024]{1,0:T(8,128)(2,1)S(1)} %collective-permute-done.1), channel_id=1, source_target_pairs={{0,3},{1,0},{2,1},{3,2},{4,7},{5,4},{6,5},{7,6},{8,11},{9,8},{10,9... | collective-permute-start | bytes 3145736 | tf_op jit(solution)/shard_map/ppermute | solution.py:44
  63.2 16.5 %copy-start.1 = (f32[512,1024]{1,0:T(8,128)S(1)}, f32[512,1024]{1,0:T(8,128)}, u32[]{:S(2)}) copy-start(f32[512,1024]{1,0:T(8,128)} %fusion.55) | copy-start | bytes 6291460
  63.2 16.5 %copy-start.2 = (f32[512,1024]{1,0:T(8,128)S(1)}, f32[512,1024]{1,0:T(8,128)}, u32[]{:S(2)}) copy-start(f32[512,1024]{1,0:T(8,128)} %fusion.53) | copy-start | bytes 6291460
  63.2 16.5 %copy-start.3 = (f32[512,1024]{1,0:T(8,128)S(1)}, f32[512,1024]{1,0:T(8,128)}, u32[]{:S(2)}) copy-start(f32[512,1024]{1,0:T(8,128)} %fusion.51) | copy-start | bytes 6291460
  68.4 18.5 %copy-start.6 = (f32[1024]{0:T(1024)S(1)}, f32[1024]{0:T(1024)}, u32[]{:S(2)}) copy-start(f32[1024]{0:T(1024)} %param.15) | copy-start | bytes 12292
  82.1 4.8 %collective-permute-start.4 = (bf16[1024,30]{0,1:T(8,128)(2,1)S(1)}, bf16[1024,30]{0,1:T(8,128)(2,1)S(1)}, u32[]{:S(2)}, u32[]{:S(2)}) collective-permute-start(bf16[1024,30]{0,1:T(8,128)(2,1)S(1)} %slice.341), channel_id=1, source_target_pairs={{0,4},{4,8},{8,12},{12,16},{16,20},{20,24},{24,28},{1,5},{5,9},{9,... | collective-permute-start | bytes 184328 | tf_op jit(solution)/shard_map/ppermute | solution.py:13
  86.9 16.6 %copy-start.8 = (f32[1024]{0:T(1024)S(1)}, f32[1024]{0:T(1024)}, u32[]{:S(2)}) copy-start(f32[1024]{0:T(1024)} %param.17) | copy-start | bytes 12292
  86.9 16.6 %copy-start.9 = (f32[1024]{0:T(1024)S(1)}, f32[1024]{0:T(1024)}, u32[]{:S(2)}) copy-start(f32[1024]{0:T(1024)} %param.16) | copy-start | bytes 12292
Sparse Core Ops, SparseCore 0:
  8.9 46.7 all-gather.2
  57.2 38.0 all-gather.4
